TPU v7x, 32 devices: a whole 2x2x4 slice. The times are simulated.
32 devices in a mesh: ep: 8 (over z, y), tp: 4 (over x, core).
Axes of the slice: x: 2, y: 2, z: 4, core: 2. Of those that a mesh axis runs over, the one named last changes fastest.
Arguments:
- queries: bfloat16 [1536, 2048], P('ep', 'tp'), may hold values from -5 to 5
- keys: bfloat16 [1536, 512], P('ep', 'tp'), may hold values from -5 to 5
- values: bfloat16 [1536, 512], P('ep', 'tp'), may hold values from -6 to 6
- query_gain: float32 [128], replicated, may hold values from 0.6 to 6
- key_gain: float32 [128], replicated, may hold values from 0.6 to 6
- out_weight: bfloat16 [2048, 2048], P('tp'), may hold values from -0.125 to 0.125
- mixer_gain: float32 [2048], replicated, may hold values from 0.1 to 1.9
- expert_in: bfloat16 [4096, 2048], P(('ep', 'tp')), may hold values from -6 to 6
- routes: int32 [4096, 2], P(('ep', 'tp')), may hold values from 0 to 7, all different within a row; in each aligned block of 128 rows (0 to 127, 128 to 255, ...) at most 48 rows name the same one
- route_weights: float32 [4096, 2], P(('ep', 'tp')), may hold values from 0.2 to 1
- expert_gain: float32 [2048], replicated, may hold values from 0.5 to 4
- gate_w: bfloat16 [8, 2048, 2048], P('ep', None, 'tp'), may hold values from -0.125 to 0.125
- up_w: bfloat16 [8, 2048, 2048], P('ep', None, 'tp'), may hold values from -0.125 to 0.125
- down_w: bfloat16 [8, 2048, 2048], P('ep', 'tp'), may hold values from -0.125 to 0.125
- ffn_out_gain: float32 [2048], replicated, may hold values from 0.1 to 1.9
Outputs:
- mixer_out: bfloat16 [1536, 2048], P(('ep', 'tp'))
- expert_out: bfloat16 [4096, 2048], P(('ep', 'tp'))
Inputs may be any that keep to these rules, and one draw needn't show every extreme that they name: `routes`: each row names 2 different experts. Among the rows of one device no expert is named by more than 48 rows, and in every draw some expert is named by exactly 48 rows of some device.
All inputs are finite; a program needn't handle non-finite values.
Results may differ from a plain program's by a relative error of at most 0.015.
The roundings to bfloat16 on the way count: a program that leaves them out, or rounds other values in their place, can miss the bound.
Values may be sent and summed in bfloat16 or wider, within the bound.
A program may use at most 128 MiB of HBM per device.

v0:
```python
import jax
import jax.numpy as jnp
from jax import lax
from jax.sharding import PartitionSpec as P

HEAD = 128
GRID_W = 64


norm_eps = 1e-06
rope_base = 10000.0
clamp_limit = 7.0
sigmoid_slope = 1.702


def rms_scale(values_in, gain):
    return (
        values_in
        * lax.rsqrt(jnp.mean(values_in * values_in, axis=-1, keepdims=True) + norm_eps)
        * gain
    )


def turn_pair(halfpart, cosine, sine):
    first_part, second_part = jnp.split(halfpart, 2, axis=-1)
    return jnp.concatenate(
        [first_part * cosine - second_part * sine, second_part * cosine + first_part * sine],
        axis=-1,
    )


def grid_rotate(field, position):
    half_width = field.shape[-1] // 2
    inverse = rope_base ** (-jnp.arange(0, half_width, 2, dtype=jnp.float32) / half_width)
    grid_row = (position // GRID_W).astype(jnp.float32)
    grid_col = (position % GRID_W).astype(jnp.float32)
    row_angle = (grid_row[:, None] * inverse[None, :])[:, None, :]
    col_angle = (grid_col[:, None] * inverse[None, :])[:, None, :]
    return jnp.concatenate(
        [
            turn_pair(field[..., :half_width], jnp.cos(row_angle), jnp.sin(row_angle)),
            turn_pair(field[..., half_width:], jnp.cos(col_angle), jnp.sin(col_angle)),
        ],
        axis=-1,
    )


def clamped_unit(gate_pre, up_pre):
    gate_cut = jnp.minimum(gate_pre, clamp_limit)
    up_cut = jnp.clip(up_pre, -clamp_limit, clamp_limit)
    return ((up_cut + 1.0) * gate_cut * jax.nn.sigmoid(sigmoid_slope * gate_cut)).astype(
        jnp.bfloat16
    )


def mixer_half(queries, keys, values, query_gain, key_gain, out_weight, mixer_gain):
    local_rows = queries.shape[0]
    kv_local = keys.shape[1] // HEAD
    group_size = queries.shape[1] // HEAD // kv_local
    position = lax.axis_index("ep") * local_rows + jnp.arange(local_rows, dtype=jnp.int32)
    query_f = queries.astype(jnp.float32).reshape(local_rows, kv_local * group_size, HEAD)
    query_norm = grid_rotate(rms_scale(query_f, query_gain), position).astype(jnp.bfloat16)
    query_norm = query_norm.reshape(local_rows, kv_local, group_size, HEAD)
    key_f = keys.astype(jnp.float32).reshape(local_rows, kv_local, HEAD)
    key_norm = grid_rotate(rms_scale(key_f, key_gain), position).astype(jnp.bfloat16)
    key_norm = key_norm.reshape(local_rows, kv_local * HEAD)
    score_scale = HEAD ** (-0.5)
    initial = (
        jnp.full((kv_local, group_size, local_rows), -1e30, jnp.float32),
        jnp.zeros((kv_local, group_size, local_rows), jnp.float32),
        jnp.zeros((kv_local, group_size, local_rows, HEAD), jnp.float32),
    )
    key_piece = lax.all_gather(key_norm, "ep", axis=0, tiled=True)
    value_piece = lax.all_gather(values, "ep", axis=0, tiled=True)
    piece_rows = key_piece.shape[0]
    block_rows = 1
    for candidate in range(min(piece_rows, 1024), 0, -1):
        if piece_rows % candidate == 0:
            block_rows = candidate
            break
    key_blocks = key_piece.reshape(piece_rows // block_rows, block_rows, kv_local, HEAD)
    value_blocks = value_piece.reshape(piece_rows // block_rows, block_rows, kv_local, HEAD)

    def one_block(state, blocks_in):
        running_max, running_total, weighted = state
        key_block, value_block = blocks_in
        scores = (
            jnp.einsum("qhgd,khd->hgqk", query_norm, key_block, preferred_element_type=jnp.float32)
            * score_scale
        )
        new_max = jnp.maximum(running_max, jnp.max(scores, axis=-1))
        factor = jnp.exp(running_max - new_max)
        expo = jnp.exp(scores - new_max[..., None])
        new_total = running_total * factor + jnp.sum(expo, axis=-1)
        new_weighted = weighted * factor[..., None] + jnp.einsum(
            "hgqk,khd->hgqd",
            expo.astype(jnp.bfloat16),
            value_block,
            preferred_element_type=jnp.float32,
        )
        return ((new_max, new_total, new_weighted), None)

    state_out, unused = lax.scan(one_block, initial, (key_blocks, value_blocks))
    final_max, final_total, weighted = state_out
    attended = (weighted / final_total[..., None]).astype(jnp.bfloat16)
    attended = jnp.transpose(attended, (2, 0, 1, 3)).reshape(
        local_rows, kv_local * group_size * HEAD
    )
    share_rows = local_rows // lax.axis_size("tp")
    selected = lax.slice_in_dim(attended, 0, lax.axis_size("tp") * share_rows, axis=0)
    projected = lax.psum_scatter(
        jnp.dot(selected, out_weight, preferred_element_type=jnp.float32).astype(jnp.bfloat16),
        "tp",
        scatter_dimension=0,
        tiled=True,
    ).astype(jnp.float32)
    return rms_scale(projected, mixer_gain).astype(jnp.bfloat16)


def expert_half(expert_in, routes, route_weights, expert_gain, gate_w, up_w, down_w, ffn_out_gain):
    tok_rows = expert_in.shape[0]
    model_width = expert_in.shape[1]
    top_count = routes.shape[1]
    expert_count = lax.axis_size("ep")
    capacity = max(2, (3 * tok_rows * top_count + 2 * expert_count - 1) // (2 * expert_count))
    normed = rms_scale(expert_in.astype(jnp.float32), expert_gain).astype(jnp.bfloat16)
    pair_expert = routes.reshape(-1)
    pair_count = pair_expert.shape[0]
    one_hot = (pair_expert[:, None] == jnp.arange(expert_count, dtype=jnp.int32)[None, :]).astype(
        jnp.int32
    )
    pair_rank = jnp.sum(jnp.cumsum(one_hot, axis=0) * one_hot, axis=1) - 1
    pair_slot = pair_expert * capacity + pair_rank
    slot_pair = (
        jnp.full((expert_count * capacity,), pair_count, jnp.int32)
        .at[pair_slot]
        .set(jnp.arange(pair_count, dtype=jnp.int32))
    )
    padded = jnp.concatenate([normed, jnp.zeros((1, model_width), jnp.bfloat16)], axis=0)
    outgoing = padded[slot_pair // top_count].reshape(expert_count, capacity, model_width)
    gate_local = gate_w[0]
    up_local = up_w[0]
    down_local = down_w[0]
    arrived = lax.all_to_all(outgoing, "ep", split_axis=0, concat_axis=0, tiled=True)
    flat_rows = arrived.reshape(-1, model_width)
    shard_rows = lax.all_gather(flat_rows, "tp", axis=0, tiled=True)
    hidden = clamped_unit(
        jnp.dot(shard_rows, gate_local, preferred_element_type=jnp.float32),
        jnp.dot(shard_rows, up_local, preferred_element_type=jnp.float32),
    )
    selected = lax.slice_in_dim(hidden, 0, lax.axis_size("tp") * flat_rows.shape[0], axis=0)
    result = lax.psum_scatter(
        jnp.dot(selected, down_local, preferred_element_type=jnp.float32).astype(jnp.bfloat16),
        "tp",
        scatter_dimension=0,
        tiled=True,
    )
    finished = result.reshape(arrived.shape)
    returned = lax.all_to_all(finished, "ep", split_axis=0, concat_axis=0, tiled=True)
    pair_result = returned.reshape(-1, model_width)[pair_slot].reshape(
        tok_rows, top_count, model_width
    )
    combined = jnp.einsum("tk,tkd->td", route_weights, pair_result.astype(jnp.float32))
    return rms_scale(combined, ffn_out_gain).astype(jnp.bfloat16)


def local(
    queries,
    keys,
    values,
    query_gain,
    key_gain,
    out_weight,
    mixer_gain,
    expert_in,
    routes,
    route_weights,
    expert_gain,
    gate_w,
    up_w,
    down_w,
    ffn_out_gain,
):
    mixer_out = mixer_half(queries, keys, values, query_gain, key_gain, out_weight, mixer_gain)
    expert_out = expert_half(
        expert_in, routes, route_weights, expert_gain, gate_w, up_w, down_w, ffn_out_gain
    )
    return (mixer_out, expert_out)


def solution(mesh):
    in_specs = (
        P("ep", "tp"),
        P("ep", "tp"),
        P("ep", "tp"),
        P(),
        P(),
        P("tp", None),
        P(),
        P(("ep", "tp"), None),
        P(("ep", "tp"), None),
        P(("ep", "tp"), None),
        P(),
        P("ep", None, "tp"),
        P("ep", None, "tp"),
        P("ep", "tp", None),
        P(),
    )
    out_specs = (P(("ep", "tp"), None), P(("ep", "tp"), None))
    return jax.shard_map(local, mesh=mesh, in_specs=in_specs, out_specs=out_specs, check_vma=False)
```

profile of v0, /device:TPU:9, one launch (start us, length us, event | category | flops | bytes accessed | tf_op | source)
XLA Modules:
  0.0 255.3 jit_solution(10198125140260231767)
XLA Ops:
  10.3 1.4 scatter_custom_fusion
  11.8 1.2 fusion.25
  13.0 1.2 fusion.27
  14.3 3.1 %gather_fusion = bf16[384,2048]{1,0:T(8,128)(2,1)} fusion(bf16[129,2048]{1,0:T(8,128)(2,1)S(1)} %concatenate.47, s32[1024]{0:T(1024)S(1)} %pad_clamp_fusion.1), kind=kCustom, calls=%fused_computation | custom fusion | bytes 3147264 | tf_op jit(solution)/shard_map/gather | solution.py:140
  17.4 41.0 %all_to_all.10 = bf16[8,48,2048]{2,1,0:T(8,128)(2,1)} all-to-all(bf16[8,48,2048]{2,1,0:T(8,128)(2,1)} %bitcast.136), channel_id=1, replica_groups=mesh['ep'=8,'tp'=4] {'ep'}, dimensions={0} | all-to-all | bytes 3145728 | tf_op jit(solution)/shard_map/all_to_all | solution.py:144
  58.7 47.5 %all-gather.2.cloned.1.call-done = bf16[1536,2048]{1,0:T(8,128)(2,1)} async-done(((bf16[384,2048]{1,0:T(8,128)(2,1)}), bf16[1536,2048]{1,0:T(8,128)(2,1)}) %all-gather.2.cloned.1.call-update) | async-done | bytes 6291472 | tf_op jit(solution)/shard_map/all_gather | solution.py:146
  106.2 8.5 %convolution_minimum_fusion = f32[1536,512]{1,0:T(8,128)} fusion(bf16[1536,2048]{1,0:T(8,128)(2,1)} %all-gather.2.cloned.1.call-done, bf16[1,2048,512]{2,1,0:T(8,128)(2,1)} %param.28), kind=kOutput, calls=%fused_computation.30 | convolution fusion | flops 3222011904 | bytes 11534336 | tf_op jit(solution)/shard_map/dot_general | solution.py:148
  114.7 11.9 %convolution_convert_fusion = bf16[1536,2048]{1,0:T(8,128)(2,1)} fusion(bf16[1,512,2048]{2,1,0:T(8,128)(2,1)S(1)} %copy-done, f32[1536,512]{1,0:T(8,128)} %convolution_minimum_fusion, bf16[1536,2048]{1,0:T(8,128)(2,1)} %all-gather.2.cloned.1.call-done, bf16[1,2048,512]{2,1,0:T(8,128)(2,1)} %param.29), kind=kOutput, calls=%fused_computation.28 | convolution fusion | flops 6452674560 | bytes 19922944 | tf_op jit(solution)/shard_map/dot_general | solution.py:153
  131.7 22.8 %all_gather.9 = bf16[1536,128]{1,0:T(8,128)(2,1)S(1)} all-gather(bf16[192,128]{1,0:T(8,128)(2,1)S(1)} %pad_maximum_fusion.1), channel_id=1, replica_groups=mesh['ep'=8,'tp'=4] {'ep'}, dimensions={0}, use_global_device_ids=true | all-gather | bytes 442368 | tf_op jit(solution)/shard_map/all_gather | solution.py:73
  154.5 25.3 %all_gather.10 = bf16[1536,128]{1,0:T(8,128)(2,1)S(1)} all-gather(bf16[192,128]{1,0:T(8,128)(2,1)S(1)} %copy-done.4), channel_id=1, replica_groups=mesh['ep'=8,'tp'=4] {'ep'}, dimensions={0}, use_global_device_ids=true | all-gather | bytes 442368 | tf_op jit(solution)/shard_map/all_gather | solution.py:74
  179.8 10.1 %while.15 = (s32[]{:T(128)}, f32[1,4,192]{2,1,0:T(4,128)S(1)}, f32[1,4,192]{2,1,0:T(4,128)S(1)}, f32[1,4,192,128]{3,2,1,0:T(8,128)S(1)}, bf16[2,768,1,128]{3,1,2...) while((s32[]{:T(128)}, f32[1,4,192]{2,1,0:T(4,128)S(1)}, ...), condition=%wide.region_5.6_spmd.clone, body=%wide.region_2.5_spmd.clone.sunk | while | flops 307008000 | bytes 17942668 | solution.py:103
  179.8 1.9 bitcast_reduce_fusion.2
  181.7 2.5 fusion.94
  184.8 1.9 bitcast_reduce_fusion.2
  186.7 2.5 fusion.94
  189.9 7.4 %all-to-all-start.1 = ((bf16[8,48,2048]{2,1,0:T(8,128)(2,1)}), bf16[8,48,2048]{2,1,0:T(8,128)(2,1)}, u32[]{:S(2)}, u32[]{:S(2)}) async-start(bf16[8,48,2048]{2,1,0:T(8,128)(2,1)} %bitcast.141), calls=%async_computation.3 | async-start | bytes 3145728 | tf_op jit(solution)/shard_map/all_to_all | solution.py:159
  197.7 3.1 %convolution_convert_fusion.1 = bf16[192,2048]{1,0:T(8,128)(2,1)} fusion(bf16[512,2048]{1,0:T(8,128)(2,1)} %param.22, bf16[24,8,4,128]{3,2,1,0:T(4,128)(2,1)S(1)} %bitcast.142), kind=kOutput, calls=%fused_computation.35 | convolution fusion | flops 403046400 | bytes 3080192 | tf_op jit(solution)/shard_map/dot_general | solution.py:112
  201.0 35.4 %reduce-scatter.3.cloned.1.call-done = bf16[48,2048]{1,0:T(8,128)(2,1)} async-done(((bf16[192,2048]{1,0:T(8,128)(2,1)}), bf16[48,2048]{1,0:T(8,128)(2,1)}) %reduce-scatter.3.cloned.1.call-update) | async-done | bytes 196624 | tf_op jit(solution)/shard_map/reduce_scatter | solution.py:111
  236.4 1.1 fusion.33
  237.5 1.7 fusion.35
  239.2 4.0 %gather_fusion.1 = bf16[256,2048]{1,0:T(8,128)(2,1)S(1)} fusion(bf16[384,2048]{1,0:T(8,128)(2,1)} %bitcast.23, s32[1024]{0:T(1024)S(1)} %pad_clamp_fusion), kind=kCustom, calls=%fused_computation.1 | custom fusion | bytes 2098176 | tf_op jit(solution)/shard_map/gather | solution.py:160
  243.2 1.5 reshape.497
  244.7 2.5 fusion.79
  247.6 1.2 fusion.30
  (82 shorter events, 10.5 us)
Async XLA Ops:
  7.2 107.6 %copy-start = (bf16[1,512,2048]{2,1,0:T(8,128)(2,1)S(1)}, bf16[1,512,2048]{2,1,0:T(8,128)(2,1)}, u32[]{:S(2)}) copy-start(bf16[1,512,2048]{2,1,0:T(8,128)(2,1)} %param.30) | copy-start | bytes 6291460
  7.2 99.0 %all-gather.2.cloned.1.call-start = ((), (), s32[]{:S(2)}) async-start(), calls=%async_computation.5 | async-start | bytes 7864320 | tf_op jit(solution)/shard_map/all_gather | solution.py:146
  58.4 131.5 %reduce-scatter.5.cloned.1.call-start = ((), (), s32[]{:S(2)}) async-start(), calls=%async_computation.6 | async-start | bytes 7864320 | tf_op jit(solution)/shard_map/reduce_scatter | solution.py:152
  126.7 0.9 copy-start.3
  126.7 2.2 copy-start.8
  128.9 1.7 copy-start.2
  128.9 1.8 copy-start.9
  129.2 25.3 %copy-start.4 = (bf16[192,128]{1,0:T(8,128)(2,1)S(1)}, bf16[192,128]{1,0:T(8,128)(2,1)}, u32[]{:S(2)}) copy-start(bf16[192,128]{1,0:T(8,128)(2,1)} %param.19) | copy-start | bytes 147460
  181.7 2.5 copy-start.1
  186.7 2.5 copy-start.1
  189.9 49.3 %all-to-all-start.1 = ((bf16[8,48,2048]{2,1,0:T(8,128)(2,1)}), bf16[8,48,2048]{2,1,0:T(8,128)(2,1)}, u32[]{:S(2)}, u32[]{:S(2)}) async-start(bf16[8,48,2048]{2,1,0:T(8,128)(2,1)} %bitcast.141), calls=%async_computation.3 | async-start | bytes 3145728 | tf_op jit(solution)/shard_map/all_to_all | solution.py:159
  197.3 39.1 %reduce-scatter.3.cloned.1.call-start = ((), (), s32[]{:S(2)}) async-start(), calls=%async_computation.4 | async-start | bytes 983040 | tf_op jit(solution)/shard_map/reduce_scatter | solution.py:111
  197.3 3.5 %copy-start.7 = (f32[128,2]{0,1:T(2,128)S(1)}, f32[128,2]{0,1:T(2,128)}, u32[]{:S(2)}) copy-start(f32[128,2]{0,1:T(2,128)} %param.26) | copy-start | bytes 3076
  197.5 40.0 %copy-start.6 = (f32[2048]{0:T(1024)S(1)}, f32[2048]{0:T(1024)}, u32[]{:S(2)}) copy-start(f32[2048]{0:T(1024)} %param.23) | copy-start | bytes 24580
  244.7 2.9 %copy-start.5 = (f32[2048]{0:T(1024)S(1)}, f32[2048]{0:T(1024)}, u32[]{:S(2)}) copy-start(f32[2048]{0:T(1024)} %param.31) | copy-start | bytes 24580
Sparse Core Ops, SparseCore 0:
  58.6 47.6 all-gather.1
  126.8 58.2 reduce-scatter.4
  200.9 35.4 reduce-scatter.2
where the time goes:
time: 258 us; the launch traced here: 255 us
  blocking collectives  89 us (34%)
  waiting for transfers between devices  83.1 us (32%)
  matrix products  34.7 us (13%)
  between operations  14.1 us (5%)
  other arithmetic  13.5 us (5%)
  local copies, waits for them, and re-layouts  13.1 us (5%)
  starting transfers between devices  7.67 us (3%)
    all_gather x1, waiting for transfers between devices, expert_half(): shard_rows = lax.all_gather(flat_rows, 'tp', axis=0, tiled=True)  47.5 us
    all_to_all x1, blocking collectives, expert_half(): lax.all_to_all(outgoing, 'ep', split_axis=0, concat_axis=0, tiled=True)  41 us
    reduce_scatter x1, waiting for transfers between devices, mixer_half(): lax.psum_scatter(jnp.dot(selected, out_weight, preferred_element_type=jnp...  35.4 us
    all_gather x1, blocking collectives, mixer_half(): value_piece = lax.all_gather(values, 'ep', axis=0, tiled=True)  25.3 us
    all_gather x1, blocking collectives, mixer_half(): key_piece = lax.all_gather(key_norm, 'ep', axis=0, tiled=True)  22.8 us
    dot_general x1, matrix products, expert_half(): jnp.dot(selected, down_local, preferred_element_type=jnp.float32)  11.9 us
    dot_general x1, matrix products, expert_half(): jnp.dot(shard_rows, gate_local, preferred_element_type=jnp.float32)  8.52 us
    all_to_all x1, starting transfers between devices, expert_half(): lax.all_to_all(finished, 'ep', split_axis=0, concat_axis=0, tiled=True)  7.41 us
  transfers between devices with their start and end apart: 4, of which 2 were waited for; matrix products, arithmetic and copies ran while one was open for 8% of the time, Pallas kernels for 0%

commit v1 on v0

--- a/solution.py
+++ b/solution.py
@@ -1,6 +1,8 @@
 import jax
 import jax.numpy as jnp
 from jax import lax
+from jax.experimental import pallas as pl
+from jax.experimental.pallas import tpu as pltpu
 from jax.sharding import PartitionSpec as P
 
 HEAD = 128
@@ -162,6 +164,538 @@
     )
     combined = jnp.einsum("tk,tkd->td", route_weights, pair_result.astype(jnp.float32))
     return rms_scale(combined, ffn_out_gain).astype(jnp.bfloat16)
+
+
+def flip(index, bits):
+    power = 1
+    while power <= bits:
+        if bits & power:
+            index = index + power - 2 * power * lax.rem(lax.div(index, power), 2)
+        power *= 2
+    return index
+
+
+def peer_order(count):
+    far = [j for j in range(count // 2, count) if j > 1]
+    near = [j for j in range(2, count // 2)]
+    order = [0, 1]
+    while far or near:
+        if far:
+            order.append(far.pop(0))
+        if near:
+            order.append(near.pop(0))
+    return order[:count]
+
+
+def capacity_of(tok_rows, top_count, expert_count):
+    return max(2, (3 * tok_rows * top_count + 2 * expert_count - 1) // (2 * expert_count))
+
+
+def fused_fits(queries, keys, expert_in, routes, gate_w):
+    n_ep, n_tp = lax.axis_size("ep"), lax.axis_size("tp")
+    rows = queries.shape[0]
+    capacity = capacity_of(expert_in.shape[0], routes.shape[1], n_ep)
+    width = expert_in.shape[1]
+    hidden = gate_w.shape[2]
+    slots = n_ep * capacity
+    held = 2 * width * slots * 14 + 6 * width * hidden * 4 + 4 * rows * rows * n_ep
+    return (
+        n_tp == 4
+        and n_ep >= 4
+        and n_ep & (n_ep - 1) == 0
+        and keys.shape[1] == HEAD
+        and capacity % 16 == 0
+        and rows % (16 * n_tp) == 0
+        and expert_in.shape[0] % 16 == 0
+        and held < 56 * 2**20
+    )
+
+
+def fused_kernel(
+    order,
+    out_ref_q,
+    kv_ref,
+    outg_ref,
+    weight_ref,
+    mixer_gain_ref,
+    ffn_gain_ref,
+    out_w_hbm,
+    gate_hbm,
+    up_hbm,
+    down_hbm,
+    mixer_out_ref,
+    expert_out_ref,
+    out_w,
+    gate,
+    up,
+    down,
+    kv_all,
+    att,
+    proj,
+    proj_in,
+    proj_sum,
+    proj_xin,
+    rows,
+    part,
+    part_in,
+    part_sum,
+    part_xin,
+    final,
+    ret,
+    w_sem,
+    own_sem,
+    kv_send,
+    kv_recv,
+    disp_send,
+    disp_recv,
+    core_send,
+    core_recv,
+    chip_send,
+    chip_recv,
+    relay_send,
+    relay_recv,
+    pcore_send,
+    pcore_recv,
+    pchip_send,
+    pchip_recv,
+    ret_send,
+    ret_recv,
+    mix_send,
+    mix_recv,
+):
+    q_ref = out_ref_q
+    n = len(order)
+    width = rows.shape[1]
+    cap = ret.shape[0] // n
+    local_rows = kv_ref.shape[0]
+    share = local_rows // 4
+    heads = q_ref.shape[0] // local_rows
+    ep, tp = lax.axis_index("ep"), lax.axis_index("tp")
+
+    def at(ref, start, size):
+        return ref.at[pl.ds(start, size), :]
+
+    def remote(src, dst, send, recv, ep_bits, tp_bits):
+        return pltpu.make_async_remote_copy(
+            src_ref=src,
+            dst_ref=dst,
+            send_sem=send,
+            recv_sem=recv,
+            device_id={"ep": flip(ep, ep_bits), "tp": flip(tp, tp_bits)},
+            device_id_type=pl.DeviceIdType.MESH,
+        )
+
+    loads = [
+        pltpu.make_async_copy(a, b, w_sem.at[i])
+        for i, (a, b) in enumerate(
+            [(gate_hbm, gate), (up_hbm, up), (down_hbm, down), (out_w_hbm, out_w)]
+        )
+    ]
+    for load in loads:
+        load.start()
+    own_kv = pltpu.make_async_copy(kv_ref, at(kv_all, 0, local_rows), own_sem.at[0])
+    own_rows = pltpu.make_async_copy(at(outg_ref, 0, cap), at(rows, 0, cap), own_sem.at[1])
+    own_kv.start()
+    own_rows.start()
+
+    barrier = pltpu.get_barrier_semaphore()
+    peers = [(j, 0) for j in range(1, n)] + [(0, 1), (0, 2)]
+    for ep_bits, tp_bits in peers:
+        pl.semaphore_signal(
+            barrier,
+            inc=1,
+            device_id={"ep": flip(ep, ep_bits), "tp": flip(tp, tp_bits)},
+            device_id_type=pl.DeviceIdType.MESH,
+        )
+    pl.semaphore_wait(barrier, len(peers))
+
+    kv_stages = []
+    held = [0]
+    bit = n // 2
+    while bit >= 1:
+        stage = []
+        for block in held:
+            source = kv_ref if block == 0 else at(kv_all, block * local_rows, local_rows)
+            slot = block + bit
+            stage.append(
+                remote(
+                    source,
+                    at(kv_all, slot * local_rows, local_rows),
+                    kv_send.at[slot],
+                    kv_recv.at[slot],
+                    bit,
+                    0,
+                )
+            )
+        kv_stages.append(stage)
+        held = held + [block + bit for block in held]
+        bit //= 2
+
+    def place(slot, which):
+        return (4 * slot + which) * cap
+
+    dispatch = [
+        None
+        if j == 0
+        else remote(
+            at(outg_ref, k * cap, cap),
+            at(rows, place(k, 0), cap),
+            disp_send.at[k],
+            disp_recv.at[k],
+            j,
+            0,
+        )
+        for k, j in enumerate(order)
+    ]
+    to_core, to_chip, relay = [], [], []
+    p_core, p_chip, give_back = [], [], []
+    for k, j in enumerate(order):
+        source = at(outg_ref, 0, cap) if j == 0 else at(rows, place(k, 0), cap)
+        to_core.append(
+            remote(source, at(rows, place(k, 2), cap), core_send.at[k], core_recv.at[k], 0, 1)
+        )
+        to_chip.append(
+            remote(source, at(rows, place(k, 1), cap), chip_send.at[k], chip_recv.at[k], 0, 2)
+        )
+        relay.append(
+            remote(
+                at(rows, place(k, 1), cap),
+                at(rows, place(k, 3), cap),
+                relay_send.at[k],
+                relay_recv.at[k],
+                0,
+                1,
+            )
+        )
+        p_core.append(
+            remote(
+                at(part, place(k, 2), 2 * cap),
+                at(part_in, 2 * k * cap, 2 * cap),
+                pcore_send.at[k],
+                pcore_recv.at[k],
+                0,
+                1,
+            )
+        )
+        p_chip.append(
+            remote(
+                at(part_sum, k * cap, cap),
+                at(part_xin, k * cap, cap),
+                pchip_send.at[k],
+                pchip_recv.at[k],
+                0,
+                2,
+            )
+        )
+        give_back.append(
+            None
+            if j == 0
+            else remote(
+                at(final, k * cap, cap),
+                at(ret, k * cap, cap),
+                ret_send.at[k],
+                ret_recv.at[k],
+                j,
+                0,
+            )
+        )
+
+    def pair(group):
+        return (2 * group, 2 * group + 1)
+
+    def forward(group):
+        for k in pair(group):
+            if dispatch[k] is not None:
+                dispatch[k].wait_recv()
+            to_chip[k].start()
+            to_core[k].start()
+
+    def pass_on(group):
+        for k in pair(group):
+            to_chip[k].wait_recv()
+            relay[k].start()
+
+    def compute(group):
+        for k in pair(group):
+            to_core[k].wait_recv()
+            relay[k].wait_recv()
+        span = pl.ds(place(2 * group, 0), 8 * cap)
+        taken = rows[span, :]
+        hidden = clamped_unit(
+            jnp.dot(taken, gate[...], preferred_element_type=jnp.float32),
+            jnp.dot(taken, up[...], preferred_element_type=jnp.float32),
+        )
+        part[span, :] = jnp.dot(hidden, down[...], preferred_element_type=jnp.float32).astype(
+            jnp.bfloat16
+        )
+        for k in pair(group):
+            p_core[k].start()
+
+    def wide(ref, start, size):
+        return ref[pl.ds(start, size), :].astype(jnp.float32)
+
+    def reduce_core(group):
+        for k in pair(group):
+            p_core[k].wait_recv()
+            part_sum[pl.ds(k * cap, cap), :] = (
+                wide(part, place(k, 1), cap) + wide(part_in, (2 * k + 1) * cap, cap)
+            ).astype(jnp.bfloat16)
+            p_chip[k].start()
+
+    def reduce_chip(group):
+        for k in pair(group):
+            p_chip[k].wait_recv()
+            summed = (
+                wide(part, place(k, 0), cap)
+                + wide(part_in, 2 * k * cap, cap)
+                + wide(part_xin, k * cap, cap)
+            ).astype(jnp.bfloat16)
+            if give_back[k] is None:
+                ret[pl.ds(k * cap, cap), :] = summed
+            else:
+                final[pl.ds(k * cap, cap), :] = summed
+                give_back[k].start()
+
+    def attend(head):
+        query = q_ref[pl.ds(head * local_rows, local_rows), :]
+        scores = lax.dot_general(
+            query,
+            kv_all[:, :HEAD],
+            (((1,), (1,)), ((), ())),
+            preferred_element_type=jnp.float32,
+        ) * (HEAD ** (-0.5))
+        expo = jnp.exp(scores - jnp.max(scores, axis=-1, keepdims=True))
+        total = jnp.sum(expo, axis=-1, keepdims=True)
+        summed = jnp.dot(
+            expo.astype(jnp.bfloat16), kv_all[:, HEAD:], preferred_element_type=jnp.float32
+        )
+        att[:, head * HEAD : (head + 1) * HEAD] = (summed / total).astype(jnp.bfloat16)
+
+    def block_of(bits):
+        return pl.multiple_of(flip(tp, bits) * share, share)
+
+    mix_core = [
+        remote(
+            at(proj, block_of(1), share),
+            at(proj_in, 0, share),
+            mix_send.at[0],
+            mix_recv.at[0],
+            0,
+            1,
+        ),
+        remote(
+            at(proj, block_of(3), share),
+            at(proj_in, share, share),
+            mix_send.at[1],
+            mix_recv.at[1],
+            0,
+            1,
+        ),
+    ]
+    mix_chip = remote(proj_sum, proj_xin, mix_send.at[2], mix_recv.at[2], 0, 2)
+
+    def project():
+        proj[...] = jnp.dot(att[...], out_w[...], preferred_element_type=jnp.float32).astype(
+            jnp.bfloat16
+        )
+        for copy in mix_core:
+            copy.start()
+
+    def mix_reduce():
+        for copy in mix_core:
+            copy.wait_recv()
+        proj_sum[...] = (wide(proj, block_of(2), share) + wide(proj_in, share, share)).astype(
+            jnp.bfloat16
+        )
+        mix_chip.start()
+
+    def mix_finish():
+        mix_chip.wait_recv()
+        summed = (
+            wide(proj, block_of(0), share)
+            + wide(proj_in, 0, share)
+            + proj_xin[...].astype(jnp.float32)
+        )
+        mixer_out_ref[...] = rms_scale(summed, mixer_gain_ref[...]).astype(jnp.bfloat16)
+
+    kv_stages[0][0].start()
+    for copy in dispatch:
+        if copy is not None:
+            copy.start()
+    for copies, later in zip(kv_stages[:-1], kv_stages[1:]):
+        if copies is kv_stages[0]:
+            own_rows.wait()
+        for copy in copies:
+            copy.wait_recv()
+        for copy in later:
+            copy.start()
+    forward(0)
+    pass_on(0)
+    loads[0].wait()
+    loads[1].wait()
+    loads[2].wait()
+    groups = n // 2
+    compute(0)
+    forward(1)
+    own_kv.wait()
+    for copy in kv_stages[-1]:
+        copy.wait_recv()
+    for head in range(heads):
+        attend(head)
+        if head == heads // 2 - 1:
+            pass_on(1)
+            reduce_core(0)
+    loads[3].wait()
+    project()
+    reduce_chip(0)
+    for group in range(1, groups):
+        if group + 1 < groups:
+            forward(group + 1)
+        compute(group)
+        if group == 1:
+            mix_reduce()
+        if group + 1 < groups:
+            pass_on(group + 1)
+        if group >= 2:
+            reduce_chip(group - 1)
+        reduce_core(group)
+    mix_finish()
+    reduce_chip(groups - 1)
+    for copy in give_back:
+        if copy is not None:
+            copy.wait_recv()
+
+    rest = weight_ref[...]
+    combined = jnp.zeros((weight_ref.shape[0], width), jnp.float32)
+    for _ in range(3):
+        piece = rest.astype(jnp.bfloat16)
+        rest = rest - piece.astype(jnp.float32)
+        combined = combined + jnp.dot(piece, ret[...], preferred_element_type=jnp.float32)
+    expert_out_ref[...] = rms_scale(combined, ffn_gain_ref[...]).astype(jnp.bfloat16)
+
+    for copy in (
+        [c for stage in kv_stages for c in stage]
+        + dispatch
+        + to_core
+        + to_chip
+        + relay
+        + p_core
+        + p_chip
+        + give_back
+        + mix_core
+        + [mix_chip]
+    ):
+        if copy is not None:
+            copy.wait_send()
+
+
+def fused_local(
+    queries,
+    keys,
+    values,
+    query_gain,
+    key_gain,
+    out_weight,
+    mixer_gain,
+    expert_in,
+    routes,
+    route_weights,
+    expert_gain,
+    gate_w,
+    up_w,
+    down_w,
+    ffn_out_gain,
+):
+    n = lax.axis_size("ep")
+    order = peer_order(n)
+    local_rows = queries.shape[0]
+    heads = queries.shape[1] // HEAD
+    tok_rows, width = expert_in.shape
+    cap = capacity_of(tok_rows, routes.shape[1], n)
+    hidden = gate_w.shape[2]
+    share = local_rows // 4
+    ep = lax.axis_index("ep")
+
+    position = ep * local_rows + jnp.arange(local_rows, dtype=jnp.int32)
+    both = jnp.concatenate([queries, keys], axis=1).astype(jnp.float32)
+    both = both.reshape(local_rows, heads + 1, HEAD)
+    gains = jnp.concatenate(
+        [jnp.broadcast_to(query_gain, (heads, HEAD)), key_gain[None]], axis=0
+    )
+    turned = grid_rotate(rms_scale(both, gains), position).astype(jnp.bfloat16)
+    query_norm = jnp.transpose(turned[:, :heads], (1, 0, 2)).reshape(heads * local_rows, HEAD)
+    key_value = jnp.concatenate([turned[:, heads], values], axis=1)
+
+    normed = rms_scale(expert_in.astype(jnp.float32), expert_gain).astype(jnp.bfloat16)
+    slot_expert = jnp.bitwise_xor(ep.astype(jnp.int32), jnp.array(order, jnp.int32))
+    named = routes[:, :, None] == slot_expert[None, None, :]
+    chosen = jnp.any(named, axis=1)
+    weight = jnp.sum(jnp.where(named, route_weights[:, :, None], 0.0), axis=1)
+    token = jnp.arange(tok_rows, dtype=jnp.int32)
+    earlier = (token[:, None] > token[None, :]).astype(jnp.bfloat16)
+    rank = jnp.dot(earlier, chosen.astype(jnp.bfloat16), preferred_element_type=jnp.float32)
+    rank = rank.astype(jnp.int32)
+    taken = chosen[:, :, None] & (rank[:, :, None] == jnp.arange(cap, dtype=jnp.int32))
+    slot_weight = jnp.where(taken, weight[:, :, None], 0.0).reshape(tok_rows, n * cap)
+    pick = taken.astype(jnp.bfloat16).reshape(tok_rows, n * cap)
+    outgoing = lax.dot_general(
+        pick, normed, (((0,), (0,)), ((), ())), preferred_element_type=jnp.float32
+    ).astype(jnp.bfloat16)
+
+    vmem = pl.BlockSpec(memory_space=pltpu.VMEM)
+    anywhere = pl.BlockSpec(memory_space=pl.ANY)
+    bf16 = jnp.bfloat16
+    dma = pltpu.SemaphoreType.DMA
+
+    def fused(*refs):
+        return fused_kernel(order, *refs)
+
+    return pl.pallas_call(
+        fused,
+        out_shape=(
+            jax.ShapeDtypeStruct((share, width), bf16),
+            jax.ShapeDtypeStruct((tok_rows, width), bf16),
+        ),
+        in_specs=[vmem] * 6 + [anywhere] * 4,
+        out_specs=(vmem, vmem),
+        scratch_shapes=[
+            pltpu.VMEM((heads * HEAD, width), bf16),
+            pltpu.VMEM((width, hidden), bf16),
+            pltpu.VMEM((width, hidden), bf16),
+            pltpu.VMEM((hidden, width), bf16),
+            pltpu.VMEM((n * local_rows, 2 * HEAD), bf16),
+            pltpu.VMEM((local_rows, heads * HEAD), bf16),
+            pltpu.VMEM((local_rows, width), bf16),
+            pltpu.VMEM((2 * share, width), bf16),
+            pltpu.VMEM((share, width), bf16),
+            pltpu.VMEM((share, width), bf16),
+            pltpu.VMEM((4 * n * cap, width), bf16),
+            pltpu.VMEM((4 * n * cap, width), bf16),
+            pltpu.VMEM((2 * n * cap, width), bf16),
+            pltpu.VMEM((n * cap, width), bf16),
+            pltpu.VMEM((n * cap, width), bf16),
+            pltpu.VMEM((n * cap, width), bf16),
+            pltpu.VMEM((n * cap, width), bf16),
+            dma((4,)),
+            dma((2,)),
+        ]
+        + [dma((n,))] * 16
+        + [dma((3,))] * 2,
+        compiler_params=pltpu.CompilerParams(
+            collective_id=0, has_side_effects=True, vmem_limit_bytes=60 * 2**20
+        ),
+    )(
+        query_norm,
+        key_value,
+        outgoing,
+        slot_weight,
+        mixer_gain[None],
+        ffn_out_gain[None],
+        out_weight,
+        gate_w[0],
+        up_w[0],
+        down_w[0],
+    )
 
 
 def local(
@@ -181,6 +715,11 @@
     down_w,
     ffn_out_gain,
 ):
+    if fused_fits(queries, keys, expert_in, routes, gate_w):
+        return fused_local(
+            queries, keys, values, query_gain, key_gain, out_weight, mixer_gain, expert_in, routes,
+            route_weights, expert_gain, gate_w, up_w, down_w, ffn_out_gain,
+        )
     mixer_out = mixer_half(queries, keys, values, query_gain, key_gain, out_weight, mixer_gain)
     expert_out = expert_half(
         expert_in, routes, route_weights, expert_gain, gate_w, up_w, down_w, ffn_out_gain

time: 258 us -> 158 us (0.61)
  Pallas kernels: 0 us -> 140 us
  blocking collectives: 89 us -> 0 us
  waiting for transfers between devices: 83.1 us -> 0 us
  matrix products: 34.7 us -> 1.96 us
  between operations: 14.1 us -> 0.8 us
  starting transfers between devices: 7.67 us -> 0 us
  local copies, waits for them, and re-layouts: 13.1 us -> 5.87 us
  other arithmetic: 13.5 us -> 7.51 us
    pallas_call x0 -> x1, Pallas kernels: none -> 140 us  [fused_local(): pl.pallas_call(fused, out_shape=(jax.ShapeDtypeStruct((share, width), bf1...]
    all_gather x2 -> x0, blocking collectives: 48 us -> none  [the longest x1 25.3 us: mixer_half(): value_piece = lax.all_gather(values, 'ep', axis=0, tiled=True)]
    all_gather x1 -> x0, waiting for transfers between devices: 47.5 us -> none  [expert_half(): shard_rows = lax.all_gather(flat_rows, 'tp', axis=0, tiled=True)]
    all_to_all x1 -> x0, blocking collectives: 41 us -> none  [expert_half(): lax.all_to_all(outgoing, 'ep', split_axis=0, concat_axis=0, tiled=True)]
    reduce_scatter x2 -> x0, waiting for transfers between devices: 35.5 us -> none  [the longest x1 35.4 us: mixer_half(): lax.psum_scatter(jnp.dot(selected, out_weight, preferred_element_type=jnp...]
    dot_general x8 -> x2, matrix products: 34.7 us -> 1.96 us  [the longest x1 1.82 us: fused_local(): lax.dot_general(pick, normed, (((0,), (0,)), ((), ())), preferred_element...]
    all_to_all x1 -> x0, starting transfers between devices: 7.41 us -> none  [expert_half(): lax.all_to_all(finished, 'ep', split_axis=0, concat_axis=0, tiled=True)]
    gather x2 -> x0, local copies, waits for them, and re-layouts: 7.1 us -> none  [the longest x1 3.97 us: expert_half(): returned.reshape(-1, model_width)[pair_slot]]
  transfers between devices with their start and end apart: 4 -> 0, of which waited for: 2 -> 0; matrix products, arithmetic and copies ran while one was open for 8% -> 0% of each run, Pallas kernels for 0% -> 0%
where the time goes in v1:
time: 158 us; the launch traced here: 156 us
  Pallas kernels  140 us (89%)
  other arithmetic  7.51 us (5%)
  local copies, waits for them, and re-layouts  5.87 us (4%)
  matrix products  1.96 us (1%)
    pallas_call x1, Pallas kernels, fused_local(): pl.pallas_call(fused, out_shape=(jax.ShapeDtypeStruct((share, width), bf1...  140 us
    unnamed x12, local copies, waits for them, and re-layouts  3.52 us

profile of v1, /device:TPU:9, one launch (start us, length us, event | category | flops | bytes accessed | tf_op | source)
XLA Modules:
  0.0 156.0 jit_solution(11970625994652262488)
XLA Ops:
  0.7 0.7 broadcast_xor_fusion
  1.4 1.2 fusion
  2.6 0.8 compare_reduce_fusion
  3.4 0.7 broadcast_in_dim.30
  4.0 0.7 pad_maximum_fusion.2
  4.7 0.8 fusion.6
  5.5 0.1 convolution_convert_fusion.1
  5.7 0.1 copy.31
  5.9 0.1 copy.30
  6.1 0.1 copy.32
  6.2 0.7 broadcast_select_fusion
  6.9 0.8 multiply_cosine_fusion.1
  7.8 0.2 copy.28
  8.1 0.2 copy.29
  8.3 0.2 multiply_multiply_fusion
  8.5 0.5 subtract_convert_fusion.1
  9.0 0.1 maximum_bitcast_fusion
  9.1 0.3 pad_maximum_fusion
  9.5 0.7 slice.14
  10.2 0.6 pad_maximum_fusion.1.refs_1_
  10.8 1.8 %convolution_convert_fusion.refs_2_ = bf16[384,2048]{1,0:T(8,128)(2,1)} fusion(pred[128,384]{1,0:T(32,128)(4,1)S(1)} %get-tuple-element.3, bf16[128,2048]{1,0:T(8,128)(2,1)S(1)} %copy-done, f32[2048]{0:T(1024)S(1)} %copy-done.4, f32[128]{0:T(128)S(1)} %add_rsqrt_fusion.1), kind=kOutput, calls=%fused_computation | convolution fusion | flops 203161600 | bytes 2155008 | tf_op jit(solution)/shard_map/dot_general | solution.py:641
  12.6 139.8 %shard_map.167 = (bf16[48,2048]{1,0:T(8,128)(2,1)}, bf16[128,2048]{1,0:T(8,128)(2,1)}) custom-call(bf16[768,128]{1,0:T(8,128)(2,1)} %bitcast.24, bf16[192,256]{1,0:T(8,128)(2,1)} %pad_maximum_fusion.1.refs_1_, bf16[384,2048]{1,0:T(8,128)(2,1)} %convolution_convert_fusion.refs_2_, f32[128,384]{1,0:T(8,128)} %get-tuple-element.2.refs_3_, f32[1,2048]{1,0:T(1,128)} %bitcast.26, ...), custom_call_target="tpu_custom_call" | custom-call | tf_op jit(solution)/shard_map/pallas_call | solution.py:653
  152.5 1.6 %copy.38 = bf16[48,2048]{1,0:T(8,128)(2,1)} copy(bf16[48,2048]{1,0:T(8,128)(2,1)} %get-tuple-element.20) | data formatting | bytes 393216
  154.1 1.9 %copy.39 = bf16[128,2048]{1,0:T(8,128)(2,1)} copy(bf16[128,2048]{1,0:T(8,128)(2,1)} %get-tuple-element.21) | data formatting | bytes 1048576
  (21 shorter events, 0.3 us)
Async XLA Ops:
  0.6 7.1 %copy-start.2 = (bf16[192,128]{1,0:T(8,128)(2,1)S(1)}, bf16[192,128]{1,0:T(8,128)(2,1)}, u32[]{:S(2)}) copy-start(bf16[192,128]{1,0:T(8,128)(2,1)} %param.17) | copy-start | bytes 147460
  0.6 7.1 %copy-start.1 = (bf16[192,512]{1,0:T(8,128)(2,1)S(1)}, bf16[192,512]{1,0:T(8,128)(2,1)}, u32[]{:S(2)}) copy-start(bf16[192,512]{1,0:T(8,128)(2,1)} %param.16) | copy-start | bytes 589828
  9.0 1.2 copy-start.3
  9.0 1.8 %copy-start = (bf16[128,2048]{1,0:T(8,128)(2,1)S(1)}, bf16[128,2048]{1,0:T(8,128)(2,1)}, u32[]{:S(2)}) copy-start(bf16[128,2048]{1,0:T(8,128)(2,1)} %param.23) | copy-start | bytes 1572868
  9.0 1.8 %copy-start.4 = (f32[2048]{0:T(1024)S(1)}, f32[2048]{0:T(1024)}, u32[]{:S(2)}) copy-start(f32[2048]{0:T(1024)} %param.26) | copy-start | bytes 24580

commit v2 on v1

--- a/solution.py
+++ b/solution.py
@@ -403,17 +403,23 @@
     def pair(group):
         return (2 * group, 2 * group + 1)
 
+    def forward_one(k):
+        if dispatch[k] is not None:
+            dispatch[k].wait_recv()
+        to_chip[k].start()
+        to_core[k].start()
+
+    def pass_on_one(k):
+        to_chip[k].wait_recv()
+        relay[k].start()
+
     def forward(group):
         for k in pair(group):
-            if dispatch[k] is not None:
-                dispatch[k].wait_recv()
-            to_chip[k].start()
-            to_core[k].start()
+            forward_one(k)
 
     def pass_on(group):
         for k in pair(group):
-            to_chip[k].wait_recv()
-            relay[k].start()
+            pass_on_one(k)
 
     def compute(group):
         for k in pair(group):
@@ -518,47 +524,54 @@
         )
         mixer_out_ref[...] = rms_scale(summed, mixer_gain_ref[...]).astype(jnp.bfloat16)
 
-    kv_stages[0][0].start()
-    for copy in dispatch:
-        if copy is not None:
-            copy.start()
+    groups = n // 2
+    for copy in kv_stages[0]:
+        copy.start()
+    dispatch[1].start()
+    for k in range(2, 4):
+        dispatch[k].start()
+    forward_one(0)
+    forward_one(1)
     for copies, later in zip(kv_stages[:-1], kv_stages[1:]):
-        if copies is kv_stages[0]:
-            own_rows.wait()
         for copy in copies:
             copy.wait_recv()
         for copy in later:
             copy.start()
-    forward(0)
-    pass_on(0)
-    loads[0].wait()
-    loads[1].wait()
-    loads[2].wait()
-    groups = n // 2
-    compute(0)
-    forward(1)
+        if copies is kv_stages[0]:
+            for k in range(4, n):
+                dispatch[k].start()
+            own_rows.wait()
+            pass_on(0)
+            for load in loads[:3]:
+                load.wait()
+            compute(0)
+            forward(1)
+            reduce_core(0)
+    pass_on(1)
     own_kv.wait()
     for copy in kv_stages[-1]:
         copy.wait_recv()
-    for head in range(heads):
-        attend(head)
-        if head == heads // 2 - 1:
-            pass_on(1)
-            reduce_core(0)
-    loads[3].wait()
-    project()
-    reduce_chip(0)
     for group in range(1, groups):
         if group + 1 < groups:
             forward(group + 1)
         compute(group)
-        if group == 1:
-            mix_reduce()
+        if group < 2:
+            reduce_chip(group - 1)
         if group + 1 < groups:
             pass_on(group + 1)
+        if group == 1:
+            for head in range(heads // 2):
+                attend(head)
+        reduce_core(group)
         if group >= 2:
             reduce_chip(group - 1)
-        reduce_core(group)
+        if group == 1:
+            for head in range(heads // 2, heads):
+                attend(head)
+            loads[3].wait()
+            project()
+        if group == 2:
+            mix_reduce()
     mix_finish()
     reduce_chip(groups - 1)
     for copy in give_back:

time: 158 us -> 123 us (0.78); the launches traced: 156 us -> 123 us
  Pallas kernels: 140 us -> 107 us
    pallas_call x1, Pallas kernels: 140 us -> 107 us  [fused_local(): pl.pallas_call(fused, out_shape=(jax.ShapeDtypeStruct((share, width), bf1...]
where the time goes in v2:
time: 123 us
  Pallas kernels  107 us (87%)
  other arithmetic  7.51 us (6%)
  local copies, waits for them, and re-layouts  5.87 us (5%)
  matrix products  1.96 us (2%)
    pallas_call x1, Pallas kernels, fused_local(): pl.pallas_call(fused, out_shape=(jax.ShapeDtypeStruct((share, width), bf1...  107 us
    unnamed x12, local copies, waits for them, and re-layouts  3.52 us

profile of v2, /device:TPU:9, one launch (start us, length us, event | category | flops | bytes accessed | tf_op | source)
XLA Modules:
  0.0 122.8 jit_solution(13774342254487313109)
XLA Ops:
  0.7 0.7 broadcast_xor_fusion
  1.4 1.2 fusion
  2.6 0.8 compare_reduce_fusion
  3.4 0.7 broadcast_in_dim.30
  4.0 0.7 pad_maximum_fusion.2
  4.7 0.8 fusion.6
  5.5 0.1 convolution_convert_fusion.1
  5.7 0.1 copy.31
  5.9 0.1 copy.30
  6.1 0.1 copy.32
  6.2 0.7 broadcast_select_fusion
  6.9 0.8 multiply_cosine_fusion.1
  7.8 0.2 copy.28
  8.1 0.2 copy.29
  8.3 0.2 multiply_multiply_fusion
  8.5 0.5 subtract_convert_fusion.1
  9.0 0.1 maximum_bitcast_fusion
  9.1 0.3 pad_maximum_fusion
  9.5 0.7 slice.14
  10.2 0.6 pad_maximum_fusion.1.refs_1_
  10.8 1.8 %convolution_convert_fusion.refs_2_ = bf16[384,2048]{1,0:T(8,128)(2,1)} fusion(pred[128,384]{1,0:T(32,128)(4,1)S(1)} %get-tuple-element.3, bf16[128,2048]{1,0:T(8,128)(2,1)S(1)} %copy-done, f32[2048]{0:T(1024)S(1)} %copy-done.4, f32[128]{0:T(128)S(1)} %add_rsqrt_fusion.1), kind=kOutput, calls=%fused_computation | convolution fusion | flops 203161600 | bytes 2155008 | tf_op jit(solution)/shard_map/dot_general | solution.py:654
  12.6 106.7 %shard_map.167 = (bf16[48,2048]{1,0:T(8,128)(2,1)}, bf16[128,2048]{1,0:T(8,128)(2,1)}) custom-call(bf16[768,128]{1,0:T(8,128)(2,1)} %bitcast.24, bf16[192,256]{1,0:T(8,128)(2,1)} %pad_maximum_fusion.1.refs_1_, bf16[384,2048]{1,0:T(8,128)(2,1)} %convolution_convert_fusion.refs_2_, f32[128,384]{1,0:T(8,128)} %get-tuple-element.2.refs_3_, f32[1,2048]{1,0:T(1,128)} %bitcast.26, ...), custom_call_target="tpu_custom_call" | custom-call | tf_op jit(solution)/shard_map/pallas_call | solution.py:666
  119.3 1.6 %copy.38 = bf16[48,2048]{1,0:T(8,128)(2,1)} copy(bf16[48,2048]{1,0:T(8,128)(2,1)} %get-tuple-element.20) | data formatting | bytes 393216
  120.9 1.9 %copy.39 = bf16[128,2048]{1,0:T(8,128)(2,1)} copy(bf16[128,2048]{1,0:T(8,128)(2,1)} %get-tuple-element.21) | data formatting | bytes 1048576
  (21 shorter events, 0.3 us)
Async XLA Ops:
  0.6 7.1 %copy-start.2 = (bf16[192,128]{1,0:T(8,128)(2,1)S(1)}, bf16[192,128]{1,0:T(8,128)(2,1)}, u32[]{:S(2)}) copy-start(bf16[192,128]{1,0:T(8,128)(2,1)} %param.17) | copy-start | bytes 147460
  0.6 7.1 %copy-start.1 = (bf16[192,512]{1,0:T(8,128)(2,1)S(1)}, bf16[192,512]{1,0:T(8,128)(2,1)}, u32[]{:S(2)}) copy-start(bf16[192,512]{1,0:T(8,128)(2,1)} %param.16) | copy-start | bytes 589828
  9.0 1.2 copy-start.3
  9.0 1.8 %copy-start = (bf16[128,2048]{1,0:T(8,128)(2,1)S(1)}, bf16[128,2048]{1,0:T(8,128)(2,1)}, u32[]{:S(2)}) copy-start(bf16[128,2048]{1,0:T(8,128)(2,1)} %param.23) | copy-start | bytes 1572868
  9.0 1.8 %copy-start.4 = (f32[2048]{0:T(1024)S(1)}, f32[2048]{0:T(1024)}, u32[]{:S(2)}) copy-start(f32[2048]{0:T(1024)} %param.26) | copy-start | bytes 24580
